TPU v7x, 256 devices: a whole 4x4x8 slice. The times are simulated.
256 devices in a mesh: kv: 32 (over z, y), tp: 8 (over x, core).
Axes of the slice: x: 4, y: 4, z: 8, core: 2. Of those that a mesh axis runs over, the one named last changes fastest.
Arguments:
- residual_in: bfloat16 [256, 2048], P(None, ('kv', 'tp')), may hold values from -14 to 14
- delta_state: float32 [256, 32, 128, 128], P('kv', 'tp'), may hold values from -1 to 1
- norm_gain_first: float32 [2048], P('kv'), may hold values from 0.1 to 1.9
- gate_first: bfloat16 [2048, 5632], P('kv', 'tp'), may hold values from -0.125 to 0.125
- up_first: bfloat16 [2048, 5632], P('kv', 'tp'), may hold values from -0.125 to 0.125
- down_first: bfloat16 [5632, 2048], P('tp', 'kv'), may hold values from -0.15625 to 0.15625
- norm_gain_mixer: float32 [2048], P('kv'), may hold values from 0.1 to 1.9
- query_weight: bfloat16 [2048, 2048], P('kv', 'tp'), may hold values from -0.125 to 0.125
- key_weight: bfloat16 [2048, 2048], P('kv', 'tp'), may hold values from -0.125 to 0.125
- value_weight: bfloat16 [2048, 4096], P('kv', 'tp'), may hold values from -0.125 to 0.125
- output_gate_weight: bfloat16 [2048, 4096], P('kv', 'tp'), may hold values from -0.125 to 0.125
- beta_weight: bfloat16 [2048, 32], P('kv'), may hold values from -0.125 to 0.125
- decay_weight: bfloat16 [2048, 32], P('kv'), may hold values from -0.125 to 0.125
- decay_rate: float32 [32], P('tp'), may hold values from -2.3 to 1.1
- decay_bias: float32 [32], P('tp'), may hold values from -1 to 1
- head_gain: float32 [128], replicated, may hold values from 0.1 to 1.9
- out_weight: bfloat16 [4096, 2048], P('tp', 'kv'), may hold values from -0.125 to 0.125
- norm_gain_second: float32 [2048], P('kv'), may hold values from 0.1 to 1.9
- gate_second: bfloat16 [2048, 5632], P('kv', 'tp'), may hold values from -0.125 to 0.125
- up_second: bfloat16 [2048, 5632], P('kv', 'tp'), may hold values from -0.125 to 0.125
- down_second: bfloat16 [5632, 2048], P('tp', 'kv'), may hold values from -0.15625 to 0.15625
Outputs:
- residual_out: bfloat16 [256, 2048], P(None, ('kv', 'tp'))
- delta_state_out: float32 [256, 32, 128, 128], P('kv', 'tp')
All inputs are finite; a program needn't handle non-finite values.
Results may differ from a plain program's by a relative error of at most 0.03.
Values may be sent and summed in bfloat16 or wider, within the bound.
No kernel may reach another device: no remote copies, remote signals or barrier semaphores. Data moves between devices by JAX's collectives and lax.ppermute only.
A program may use at most 64 MiB of HBM per device.

v0:
```python
import jax
import jax.numpy as jnp
from jax import lax
from jax.sharding import Mesh
from jax.sharding import PartitionSpec as P

D = 2048
HEAD = 128
GATES = 128
epsilon = 1e-06
TP = ("x", "c")
ACROSS = ("z", "x", "c")
bf16 = jnp.bfloat16
f32 = jnp.float32


def exchange(blocks, axis):
    return lax.all_to_all(blocks, axis, split_axis=0, concat_axis=0, tiled=True)


def from_everyone(value, axis):
    return exchange(jnp.broadcast_to(value, (lax.axis_size(axis), *value.shape)), axis)


def everyone_sum(value, axis):
    return from_everyone(value, axis).astype(f32).sum(axis=0)


def times_transposed(left, right_rows):
    return lax.dot_general(left, right_rows, (((1,), (1,)), ((), ())), preferred_element_type=f32)


def square_columns(as_float):
    squares = jnp.sum(as_float * as_float, axis=1, keepdims=True)
    high = squares.astype(bf16).astype(f32)
    lane = lax.broadcasted_iota(jnp.int32, (squares.shape[0], GATES), 1)
    return jnp.where(lane == 0, high, jnp.where(lane == 1, squares - high, 0.0))


def row_scale(first_two):
    return lax.rsqrt((first_two[:, :1] + first_two[:, 1:2]) / D + epsilon)


def hidden_units(residual, gate_up):
    partial_value = jnp.dot(residual, gate_up, preferred_element_type=f32)
    both = jnp.concatenate([partial_value, square_columns(residual.astype(f32))], axis=1).astype(
        bf16
    )
    summed = everyone_sum(both, "y")
    width = gate_up.shape[1]
    scale = row_scale(summed[:, width:])
    gate_act = summed[:, : width // 2] * scale
    up_act = summed[:, width // 2 : width] * scale
    return (jax.nn.silu(gate_act) * up_act).astype(bf16)


def unit_heads(projected, head_size):
    activated = jax.nn.silu(projected).reshape(projected.shape[0], -1, head_size)
    return activated * lax.rsqrt(jnp.sum(activated * activated, axis=-1, keepdims=True) + epsilon)


def delta_step(old_state, key_rows, queries, values, beta_gate, decay_gate):
    faded_state = old_state * decay_gate[:, :, None, None]
    predicted = jnp.einsum("rhab,rha->rhb", faded_state, key_rows, precision=lax.Precision.HIGHEST)
    correction = beta_gate[:, :, None] * (values - predicted)
    updated = faded_state + key_rows[:, :, :, None] * correction[:, :, None, :]
    reading = jnp.einsum("rhab,rha->rhb", updated, queries, precision=lax.Precision.HIGHEST)
    return (updated, reading)


def mixer_values(residual, mixer_in, decay_rate, decay_bias, head_gain, old_state):
    row_count, heads_dev, head_size = old_state.shape[:3]
    projected = jnp.dot(residual, mixer_in, preferred_element_type=f32)
    width = mixer_in.shape[1] - GATES
    squares = square_columns(residual.astype(f32))
    tail = projected[:, width:] + jnp.roll(squares, 2 * heads_dev, axis=1)
    both = jnp.concatenate([projected[:, :width], tail], axis=1).astype(bf16)
    blocks = both.reshape(-1, row_count, both.shape[1])
    summed = exchange(blocks, "y").astype(f32).sum(axis=0)
    tail = summed[:, width:]
    scale = row_scale(tail[:, 2 * heads_dev :])
    summed = summed[:, :width] * scale
    gates = tail * scale
    value_cols = heads_dev * head_size
    key_cols = (width - 2 * value_cols) // 2
    repeat_count = value_cols // key_cols
    queries = jnp.repeat(
        unit_heads(summed[:, :key_cols], head_size) * head_size ** (-0.5), repeat_count, axis=1
    )
    key_rows = jnp.repeat(
        unit_heads(summed[:, key_cols : 2 * key_cols], head_size), repeat_count, axis=1
    )
    values = jax.nn.silu(summed[:, 2 * key_cols : 2 * key_cols + value_cols]).reshape(
        row_count, heads_dev, head_size
    )
    out_gate = jax.nn.silu(summed[:, 2 * key_cols + value_cols :]).reshape(
        row_count, heads_dev, head_size
    )
    beta_gate = jax.nn.sigmoid(gates[:, :heads_dev])
    decay_gate = jnp.exp(
        -jnp.exp(decay_rate)[None, :]
        * jax.nn.softplus(gates[:, heads_dev : 2 * heads_dev] + decay_bias[None, :])
    )
    new_state, reading = delta_step(old_state, key_rows, queries, values, beta_gate, decay_gate)
    normed = reading * lax.rsqrt(jnp.mean(reading * reading, axis=-1, keepdims=True) + epsilon)
    normed = (normed * head_gain * out_gate).reshape(row_count, value_cols).astype(bf16)
    return (normed, new_state)


def body(
    residual_in,
    delta_state,
    norm_gain_first,
    gate_first,
    up_first,
    down_first,
    norm_gain_mixer,
    query_weight,
    key_weight,
    value_weight,
    output_gate_weight,
    beta_weight,
    decay_weight,
    decay_rate,
    decay_bias,
    head_gain,
    out_weight,
    norm_gain_second,
    gate_second,
    up_second,
    down_second,
):
    planes, tp_count = (lax.axis_size("z"), lax.axis_size(TP))
    heads_dev = decay_rate.shape[0]

    def scaled_rows(gain, weights):
        return (jnp.concatenate(weights, axis=1).astype(f32) * gain[:, None]).astype(bf16)

    def gathered(weights):
        return lax.all_gather(jnp.concatenate(weights, axis=1), "z", axis=0, tiled=True)

    head_start = lax.axis_index(TP) * heads_dev
    gate_cols = [
        lax.dynamic_slice_in_dim(beta_weight, head_start, heads_dev, 1),
        lax.dynamic_slice_in_dim(decay_weight, head_start, heads_dev, 1),
        jnp.zeros((beta_weight.shape[0], GATES - 2 * heads_dev), bf16),
    ]
    first_in = scaled_rows(norm_gain_first, [gate_first, up_first])
    mixer_in = scaled_rows(
        norm_gain_mixer, [query_weight, key_weight, value_weight, output_gate_weight, *gate_cols]
    )
    second_in = scaled_rows(norm_gain_second, [gate_second, up_second])
    width, mixer_width = (first_in.shape[1], mixer_in.shape[1])
    first_in = gathered([first_in])
    middle = gathered([down_first.T, mixer_in])
    last = gathered([out_weight.T, second_in, down_second.T])
    down_first, mixer_in = (middle[:, : width // 2], middle[:, width // 2 :])
    values_width = out_weight.shape[0]
    out_rows, second_in, down_second = (
        last[:, :values_width],
        last[:, values_width : values_width + width],
        last[:, values_width + width :],
    )
    columns = residual_in.T
    own_cols, rows = (columns.shape[0], columns.shape[1] // planes)
    pieces = jnp.moveaxis(columns.reshape(own_cols, planes, rows), 1, 0)
    pieces = jnp.broadcast_to(pieces[:, None], (planes, tp_count, own_cols, rows))
    residual = exchange(pieces.reshape(-1, own_cols, rows), ACROSS).reshape(-1, rows).T
    hidden = hidden_units(residual, first_in)
    projected = times_transposed(hidden, down_first).astype(bf16)
    after_first = (residual.astype(f32) + 0.5 * everyone_sum(projected, TP)).astype(bf16)
    normed, new_state = mixer_values(
        after_first, mixer_in, decay_rate, decay_bias, head_gain, delta_state
    )
    normed = from_everyone(normed, "y").reshape(rows, -1)
    projected = times_transposed(normed, out_rows).astype(bf16)
    after_mixer = (after_first.astype(f32) + everyone_sum(projected, TP)).astype(bf16)
    hidden = hidden_units(after_mixer, second_in)
    projected = times_transposed(down_second, hidden).astype(bf16)
    pieces = jnp.concatenate([projected, after_mixer.T], axis=1)
    arrived = exchange(pieces.reshape(-1, own_cols, 2 * rows), ACROSS)
    arrived = arrived.reshape(planes, tp_count, own_cols, 2 * rows).astype(f32)
    final = arrived[:, 0, :, rows:] + 0.5 * arrived[..., :rows].sum(axis=1)
    residual_out = jnp.moveaxis(final, 1, 2).reshape(planes * rows, own_cols).astype(bf16)
    return (residual_out, new_state)


def solution(mesh):
    cut = Mesh(mesh.devices.reshape(8, 4, 4, 2), ("z", "y", "x", "c"))
    kv, tp = (("z", "y"), ("x", "c"))
    wide, tall = (P(kv, tp), P(tp, kv))
    placed = (
        P(None, kv + tp),
        P(kv, tp, None, None),
        P(kv),
        wide,
        wide,
        tall,
        P(kv),
        wide,
        wide,
        wide,
        wide,
        P(kv, None),
        P(kv, None),
        P(tp),
        P(tp),
        P(),
        tall,
        P(kv),
        wide,
        wide,
        tall,
    )
    return jax.shard_map(
        body,
        mesh=cut,
        in_specs=placed,
        out_specs=(P(None, kv + tp), P(kv, tp, None, None)),
        check_vma=False,
    )
```

profile of v0, /device:TPU:1, one launch (start us, length us, event | category | flops | bytes accessed | tf_op | source)
XLA Modules:
  0.0 199.8 jit_solution(17900534135852283089)
XLA Ops:
  7.2 1.7 multiply_convert_fusion.1
  9.0 0.7 constant_dynamic-slice_fusion
  9.7 0.1 copy.77
  10.0 1.0 concatenate.43
  11.0 0.8 multiply_convert_fusion
  11.7 1.8 pad_maximum_fusion.1
  13.7 0.7 reshape.127
  14.4 13.0 %all-to-all-start = ((bf16[64,2,128]{2,1,0:T(2,128)(2,1)}), bf16[64,2,128]{2,1,0:T(2,128)(2,1)S(1)}, u32[]{:S(2)}, u32[]{:S(2)}) async-start(bf16[64,2,128]{2,1,0:T(2,128)(2,1)} %reshape.127), calls=%async_computation | async-start | bytes 65536 | tf_op jit(solution)/shard_map/all_to_all | solution.py:18
  27.4 9.5 %all-to-all-done = bf16[64,2,128]{2,1,0:T(2,128)(2,1)S(1)} async-done(((bf16[64,2,128]{2,1,0:T(2,128)(2,1)}), bf16[64,2,128]{2,1,0:T(2,128)(2,1)S(1)}, u32[]{:S(2)}, u32[]{:S(2)}) %all-to-all-start) | async-done | bytes 32800 | tf_op jit(solution)/shard_map/all_to_all | solution.py:18
  37.1 0.1 fusion.19
  37.3 12.2 %all-gather.6.cloned.1.call-done = bf16[512,1408]{1,0:T(8,128)(2,1)} async-done(((bf16[64,1408]{1,0:T(8,128)(2,1)}), bf16[512,1408]{1,0:T(8,128)(2,1)}) %all-gather.6.cloned.1.call-update) | async-done | bytes 1441808 | tf_op jit(solution)/shard_map/all_gather | solution.py:140
  49.6 1.7 fusion
  51.3 0.8 broadcast_in_dim.91
  52.1 4.2 %all-to-all-start.1 = ((bf16[4,32,1536]{2,1,0:T(8,128)(2,1)}), bf16[4,32,1536]{2,1,0:T(8,128)(2,1)S(1)}, u32[]{:S(2)}, u32[]{:S(2)}) async-start(bf16[4,32,1536]{2,1,0:T(8,128)(2,1)} %broadcast_in_dim.91), calls=%async_computation.1 | async-start | bytes 786432 | tf_op jit(solution)/shard_map/all_to_all | solution.py:18
  56.4 6.1 %all-to-all-done.1 = bf16[4,32,1536]{2,1,0:T(8,128)(2,1)S(1)} async-done(((bf16[4,32,1536]{2,1,0:T(8,128)(2,1)}), bf16[4,32,1536]{2,1,0:T(8,128)(2,1)S(1)}, u32[]{:S(2)}, u32[]{:S(2)}) %all-to-all-start.1) | async-done | bytes 393248 | tf_op jit(solution)/shard_map/all_to_all | solution.py:18
  62.6 0.2 fusion.41
  62.8 29.2 %all-gather.8.cloned.1.call-done = bf16[512,2368]{1,0:T(8,128)(2,1)} async-done(((bf16[64,2368]{1,0:T(8,128)(2,1)}), bf16[512,2368]{1,0:T(8,128)(2,1)}) %all-gather.8.cloned.1.call-update) | async-done | bytes 2424848 | tf_op jit(solution)/shard_map/all_gather | solution.py:140
  91.9 1.5 convolution_convert_fusion.3
  93.4 0.7 broadcast_in_dim.93
  94.2 8.7 %all-to-all-start.2 = ((bf16[8,32,512]{2,1,0:T(8,128)(2,1)}), bf16[8,32,512]{2,1,0:T(8,128)(2,1)S(1)}, u32[]{:S(2)}, u32[]{:S(2)}) async-start(bf16[8,32,512]{2,1,0:T(8,128)(2,1)} %broadcast_in_dim.93), calls=%async_computation.2 | async-start | bytes 524288 | tf_op jit(solution)/shard_map/all_to_all | solution.py:18
  102.9 0.8 pad_maximum_fusion
  103.7 5.7 %all-to-all-done.2 = bf16[8,32,512]{2,1,0:T(8,128)(2,1)S(1)} async-done(((bf16[8,32,512]{2,1,0:T(8,128)(2,1)}), bf16[8,32,512]{2,1,0:T(8,128)(2,1)S(1)}, u32[]{:S(2)}, u32[]{:S(2)}) %all-to-all-start.2) | async-done | bytes 262176 | tf_op jit(solution)/shard_map/all_to_all | solution.py:18
  109.4 0.1 fusion.17
  109.6 2.2 %fusion.3 = f32[32,1664]{1,0:T(8,128)S(1)} fusion(bf16[32,512]{1,0:T(8,128)(2,1)S(1)} %get-tuple-element.5, bf16[512,2368]{1,0:T(8,128)(2,1)} %all-gather.8.cloned.1.call-done), kind=kOutput, calls=%fused_computation.6 | convolution fusion | flops 54525952 | bytes 1949696 | tf_op jit(solution)/shard_map/dot_general | solution.py:73
  111.9 0.7 pad_maximum_fusion.2
  112.6 4.0 %all-to-all-start.3 = ((bf16[4,8,1664]{2,1,0:T(8,128)(2,1)}), bf16[4,8,1664]{2,1,0:T(8,128)(2,1)S(1)}, u32[]{:S(2)}, u32[]{:S(2)}) async-start(bf16[4,8,1664]{2,1,0:T(8,128)(2,1)} %pad_maximum_fusion.2), calls=%async_computation.3 | async-start | bytes 212992 | tf_op jit(solution)/shard_map/all_to_all | solution.py:18
  116.6 4.7 %all-to-all-done.3 = bf16[4,8,1664]{2,1,0:T(8,128)(2,1)S(1)} async-done(((bf16[4,8,1664]{2,1,0:T(8,128)(2,1)}), bf16[4,8,1664]{2,1,0:T(8,128)(2,1)S(1)}, u32[]{:S(2)}, u32[]{:S(2)}) %all-to-all-start.3) | async-done | bytes 106528 | tf_op jit(solution)/shard_map/all_to_all | solution.py:18
  121.4 0.2 fusion.56
  122.1 2.0 %fusion.1 = f32[8,4,1,128]{3,2,1,0:T(1,128)S(1)} fusion(f32[8,4,128,1]{2,3,1,0:T(1,128)S(1)} %bitcast.109, f32[8,4,128,128]{3,2,1,0:T(8,128)S(1)} %copy-done, f32[8,4]{1,0:T(8,128)S(1)} %get-tuple-element.9), kind=kOutput, calls=%fused_computation.4 | convolution fusion | flops 6815744 | bytes 2130048 | tf_op jit(solution)/shard_map/rhab,rha->rhb/dot_general | solution.py:64
  124.2 0.8 multiply_add_fusion
  125.0 1.3 copy-done.1
  126.3 1.9 fusion.65
  128.4 6.7 %all_to_all.40 = bf16[4,8,512]{2,1,0:T(8,128)(2,1)S(1)} all-to-all(bf16[4,8,512]{2,1,0:T(8,128)(2,1)S(1)} %broadcast_in_dim.98), channel_id=1, replica_groups=mesh['z'=8,'y'=4,'x'=4,'c'=2] {'y'}, dimensions={0} | all-to-all | bytes 65536 | tf_op jit(solution)/shard_map/all_to_all | solution.py:18
  135.1 8.7 %all-gather.4.cloned.1.call-done = bf16[512,2624]{1,0:T(8,128)(2,1)} async-done(((bf16[64,2624]{1,0:T(8,128)(2,1)}), bf16[512,2624]{1,0:T(8,128)(2,1)}) %all-gather.4.cloned.1.call-update) | async-done | bytes 2686992 | tf_op jit(solution)/shard_map/all_gather | solution.py:140
  143.8 1.3 convolution_convert_fusion.4
  145.2 13.9 %all_to_all.41 = bf16[8,32,512]{2,1,0:T(8,128)(2,1)S(1)} all-to-all(bf16[8,32,512]{2,1,0:T(8,128)(2,1)S(1)} %broadcast_in_dim.99), channel_id=1, replica_groups=mesh['z'=8,'y'=4,'x'=4,'c'=2] {'x','c'}, dimensions={0} | all-to-all | bytes 524288 | tf_op jit(solution)/shard_map/all_to_all | solution.py:18
  159.1 0.1 multiply_reduce_fusion
  159.4 1.7 convolution_convert_fusion
  161.1 0.8 broadcast_in_dim.102
  161.9 3.8 %all-to-all-start.6 = ((bf16[4,32,1536]{2,1,0:T(8,128)(2,1)}), bf16[4,32,1536]{2,1,0:T(8,128)(2,1)S(1)}, u32[]{:S(2)}, u32[]{:S(2)}) async-start(bf16[4,32,1536]{2,1,0:T(8,128)(2,1)} %broadcast_in_dim.102), calls=%async_computation.6 | async-start | bytes 786432 | tf_op jit(solution)/shard_map/all_to_all | solution.py:18
  165.7 6.5 %all-to-all-done.6 = bf16[4,32,1536]{2,1,0:T(8,128)(2,1)S(1)} async-done(((bf16[4,32,1536]{2,1,0:T(8,128)(2,1)}), bf16[4,32,1536]{2,1,0:T(8,128)(2,1)S(1)}, u32[]{:S(2)}, u32[]{:S(2)}) %all-to-all-start.6) | async-done | bytes 393248 | tf_op jit(solution)/shard_map/all_to_all | solution.py:18
  172.3 0.2 fusion.36
  172.5 1.5 convolution_convert_fusion.2
  174.0 0.1 copy.83
  174.2 0.2 reshape.129
  174.3 18.0 %all_to_all.42 = bf16[64,2,256]{2,1,0:T(2,128)(2,1)S(1)} all-to-all(bf16[64,2,256]{2,1,0:T(2,128)(2,1)S(1)} %reshape.129), channel_id=1, replica_groups=mesh['z'=8,'y'=4,'x'=4,'c'=2] {'z','x','c'}, dimensions={0} | all-to-all | bytes 131072 | tf_op jit(solution)/shard_map/all_to_all | solution.py:18
  192.3 0.1 reshape.130
  192.6 0.7 convert_element_type.209
  (80 shorter events, 2.4 us)
Async XLA Ops:
  7.2 6.4 %copy-start.6 = (bf16[256,8]{0,1:T(8,128)(2,1)S(1)}, bf16[256,8]{0,1:T(8,128)(2,1)}, u32[]{:S(2)}) copy-start(bf16[256,8]{0,1:T(8,128)(2,1)} %param.21) | copy-start | bytes 12292
  7.2 42.4 %all-gather.6.cloned.1.call-start = ((), (), s32[]{:S(2)}) async-start(), calls=%async_computation.9 | async-start | bytes 1622016 | tf_op jit(solution)/shard_map/all_gather | solution.py:140
  9.0 83.0 %all-gather.8.cloned.1.call-start = ((), (), s32[]{:S(2)}) async-start(), calls=%async_computation.10 | async-start | bytes 2801664 | tf_op jit(solution)/shard_map/all_gather | solution.py:140
  13.5 42.8 %copy-start.2 = (bf16[64,704]{1,0:T(8,128)(2,1)S(1)}, bf16[64,704]{1,0:T(8,128)(2,1)}, u32[]{:S(2)}) copy-start(bf16[64,704]{1,0:T(8,128)(2,1)} %param.40) | copy-start | bytes 270340
  13.5 42.8 %copy-start.3 = (bf16[64,704]{1,0:T(8,128)(2,1)S(1)}, bf16[64,704]{1,0:T(8,128)(2,1)}, u32[]{:S(2)}) copy-start(bf16[64,704]{1,0:T(8,128)(2,1)} %param.39) | copy-start | bytes 270340
  13.5 42.8 %copy-start.7 = (f32[64]{0:T(128)S(1)}, f32[64]{0:T(128)}, u32[]{:S(2)}) copy-start(f32[64]{0:T(128)} %param.38) | copy-start | bytes 772
  14.4 22.5 %all-to-all-start = ((bf16[64,2,128]{2,1,0:T(2,128)(2,1)}), bf16[64,2,128]{2,1,0:T(2,128)(2,1)S(1)}, u32[]{:S(2)}, u32[]{:S(2)}) async-start(bf16[64,2,128]{2,1,0:T(2,128)(2,1)} %reshape.127), calls=%async_computation | async-start | bytes 65536 | tf_op jit(solution)/shard_map/all_to_all | solution.py:18
  52.1 50.8 %copy-start.4 = (bf16[704,64]{0,1:T(8,128)(2,1)S(1)}, bf16[704,64]{0,1:T(8,128)(2,1)}, u32[]{:S(2)}) copy-start(bf16[704,64]{0,1:T(8,128)(2,1)} %param.41) | copy-start | bytes 270340
  52.1 50.8 %copy-start.5 = (bf16[512,64]{0,1:T(8,128)(2,1)S(1)}, bf16[512,64]{0,1:T(8,128)(2,1)}, u32[]{:S(2)}) copy-start(bf16[512,64]{0,1:T(8,128)(2,1)} %param.37) | copy-start | bytes 196612
  52.1 10.5 %all-to-all-start.1 = ((bf16[4,32,1536]{2,1,0:T(8,128)(2,1)}), bf16[4,32,1536]{2,1,0:T(8,128)(2,1)S(1)}, u32[]{:S(2)}, u32[]{:S(2)}) async-start(bf16[4,32,1536]{2,1,0:T(8,128)(2,1)} %broadcast_in_dim.91), calls=%async_computation.1 | async-start | bytes 786432 | tf_op jit(solution)/shard_map/all_to_all | solution.py:18
  94.2 15.2 %all-to-all-start.2 = ((bf16[8,32,512]{2,1,0:T(8,128)(2,1)}), bf16[8,32,512]{2,1,0:T(8,128)(2,1)S(1)}, u32[]{:S(2)}, u32[]{:S(2)}) async-start(bf16[8,32,512]{2,1,0:T(8,128)(2,1)} %broadcast_in_dim.93), calls=%async_computation.2 | async-start | bytes 524288 | tf_op jit(solution)/shard_map/all_to_all | solution.py:18
  102.9 13.7 %copy-start.10 = (f32[4]{0:T(128)S(1)}, f32[4]{0:T(128)}, u32[]{:S(2)}) copy-start(f32[4]{0:T(128)} %param.34) | copy-start | bytes 52
  102.9 41.0 %all-gather.4.cloned.1.call-start = ((), (), s32[]{:S(2)}) async-start(), calls=%async_computation.8 | async-start | bytes 3096576 | tf_op jit(solution)/shard_map/all_gather | solution.py:140
  103.6 18.3 %copy-start.9 = (f32[4]{0:T(128)S(1)}, f32[4]{0:T(128)}, u32[]{:S(2)}) copy-start(f32[4]{0:T(128)} %param.35) | copy-start | bytes 52
  103.6 18.5 %copy-start = (f32[8,4,128,128]{3,2,1,0:T(8,128)S(1)}, f32[8,4,128,128]{3,2,1,0:T(8,128)}, u32[]{:S(2)}) copy-start(f32[8,4,128,128]{3,2,1,0:T(8,128)} %param.22) | copy-start | bytes 6291460
  112.6 8.8 %all-to-all-start.3 = ((bf16[4,8,1664]{2,1,0:T(8,128)(2,1)}), bf16[4,8,1664]{2,1,0:T(8,128)(2,1)S(1)}, u32[]{:S(2)}, u32[]{:S(2)}) async-start(bf16[4,8,1664]{2,1,0:T(8,128)(2,1)} %pad_maximum_fusion.2), calls=%async_computation.3 | async-start | bytes 212992 | tf_op jit(solution)/shard_map/all_to_all | solution.py:18
  125.0 1.3 copy-start.1
  125.0 3.3 %copy-start.8 = (f32[128]{0:T(128)S(1)}, f32[128]{0:T(128)}, u32[]{:S(2)}) copy-start(f32[128]{0:T(128)} %param.36) | copy-start | bytes 1540
  161.9 10.4 %all-to-all-start.6 = ((bf16[4,32,1536]{2,1,0:T(8,128)(2,1)}), bf16[4,32,1536]{2,1,0:T(8,128)(2,1)S(1)}, u32[]{:S(2)}, u32[]{:S(2)}) async-start(bf16[4,32,1536]{2,1,0:T(8,128)(2,1)} %broadcast_in_dim.102), calls=%async_computation.6 | async-start | bytes 786432 | tf_op jit(solution)/shard_map/all_to_all | solution.py:18
Sparse Core Ops, SparseCore 0:
  10.3 39.1 all-gather.5
  51.3 40.5 all-gather.7
  105.4 38.3 all-gather.3
where the time goes:
time: 201 us; the launch traced here: 200 us
  waiting for transfers between devices  82.7 us (41%)
  blocking collectives  38.6 us (19%)
  starting transfers between devices  33.8 us (17%)
  between operations  14.1 us (7%)
  matrix products  13.8 us (7%)
  other arithmetic  8.8 us (4%)
  local copies, waits for them, and re-layouts  7.98 us (4%)
    all_gather x3, waiting for transfers between devices, gathered(): lax.all_gather(jnp.concatenate(weights, axis=1), 'z', axis=0, tiled=True)  50.1 us
    all_to_all x3, blocking collectives, exchange(): return lax.all_to_all(blocks, axis, split_axis=0, concat_axis=0, tiled=True)  38.6 us
    all_to_all x5, starting transfers between devices, exchange(): return lax.all_to_all(blocks, axis, split_axis=0, concat_axis=0, tiled=True)  33.7 us
    all_to_all x5, waiting for transfers between devices, exchange(): return lax.all_to_all(blocks, axis, split_axis=0, concat_axis=0, tiled=True)  32.6 us
    dot_general x3, matrix products, times_transposed(): lax.dot_general(left, right_rows, (((1,), (1,)), ((), ())), preferred_ele...  4.25 us
  transfers between devices with their start and end apart: 8, of which 8 were waited for; matrix products, arithmetic and copies ran while one was open for 9% of the time, Pallas kernels for 0%

commit v1 on v0

--- a/solution.py
+++ b/solution.py
@@ -137,7 +137,12 @@
         return (jnp.concatenate(weights, axis=1).astype(f32) * gain[:, None]).astype(bf16)
 
     def gathered(weights):
-        return lax.all_gather(jnp.concatenate(weights, axis=1), "z", axis=0, tiled=True)
+        return jnp.concatenate(
+            lax.all_to_all(
+                jnp.stack([jnp.concatenate(weights, axis=1)] * lax.axis_size("z")), "z", 0, 0
+            ),
+            axis=0,
+        )
 
     head_start = lax.axis_index(TP) * heads_dev
     gate_cols = [

time: 201 us -> 289 us (1.44)
  blocking collectives: 38.6 us -> 93 us
  waiting for transfers between devices: 82.7 us -> 128 us
  between operations: 14.1 us -> 1.19 us
  starting transfers between devices: 33.8 us -> 41.3 us
  matrix products: 13.8 us -> 7.73 us
  local copies, waits for them, and re-layouts: 7.98 us -> 11.9 us
  other arithmetic: 8.8 us -> 5.11 us
    all_to_all x0 -> x2, waiting for transfers between devices: none -> 91.2 us  [gathered(): lax.all_to_all(jnp.stack([jnp.concatenate(weights, axis=1)] * lax.axis_si...]
    all_to_all x0 -> x1, blocking collectives: none -> 64.1 us  [gathered(): lax.all_to_all(jnp.stack([jnp.concatenate(weights, axis=1)] * lax.axis_si...]
    all_gather x3 -> x0, waiting for transfers between devices: 50.1 us -> none  [gathered(): lax.all_gather(jnp.concatenate(weights, axis=1), 'z', axis=0, tiled=True)]
    all_to_all x3 -> x2, blocking collectives: 38.6 us -> 28.9 us  [exchange(): return lax.all_to_all(blocks, axis, split_axis=0, concat_axis=0, tiled=True)]
    all_to_all x0 -> x2, starting transfers between devices: none -> 7.6 us  [gathered(): lax.all_to_all(jnp.stack([jnp.concatenate(weights, axis=1)] * lax.axis_si...]
    all_to_all x5 -> x6, waiting for transfers between devices: 32.6 us -> 36.3 us  [exchange(): return lax.all_to_all(blocks, axis, split_axis=0, concat_axis=0, tiled=True)]
    dot_general x3, matrix products: 4.25 us -> 0.94 us  [times_transposed(): lax.dot_general(left, right_rows, (((1,), (1,)), ((), ())), preferred_ele...]
    another operation x0 -> x3, local copies, waits for them, and re-layouts: none -> 3.05 us  [gathered(): jnp.stack([jnp.concatenate(weights, axis=1)] * lax.axis_size('z'))]
  transfers between devices with their start and end apart: 8 -> 8, of which waited for: 8 -> 8; matrix products, arithmetic and copies ran while one was open for 9% -> 1% of each run, Pallas kernels for 0% -> 0%
where the time goes in v1:
time: 289 us; the launch traced here: 288 us
  waiting for transfers between devices  128 us (44%)
  blocking collectives  93 us (32%)
  starting transfers between devices  41.3 us (14%)
  local copies, waits for them, and re-layouts  11.9 us (4%)
  matrix products  7.73 us (3%)
  other arithmetic  5.11 us (2%)
    all_to_all x2, waiting for transfers between devices, gathered(): lax.all_to_all(jnp.stack([jnp.concatenate(weights, axis=1)] * lax.axis_si...  91.2 us
    all_to_all x1, blocking collectives, gathered(): lax.all_to_all(jnp.stack([jnp.concatenate(weights, axis=1)] * lax.axis_si...  64.1 us
    all_to_all x6, waiting for transfers between devices, exchange(): return lax.all_to_all(blocks, axis, split_axis=0, concat_axis=0, tiled=True)  36.3 us
    all_to_all x6, starting transfers between devices, exchange(): return lax.all_to_all(blocks, axis, split_axis=0, concat_axis=0, tiled=True)  33.7 us
    all_to_all x2, blocking collectives, exchange(): return lax.all_to_all(blocks, axis, split_axis=0, concat_axis=0, tiled=True)  28.9 us
    all_to_all x2, starting transfers between devices, gathered(): lax.all_to_all(jnp.stack([jnp.concatenate(weights, axis=1)] * lax.axis_si...  7.6 us
  transfers between devices with their start and end apart: 8, of which 8 were waited for; matrix products, arithmetic and copies ran while one was open for 1% of the time, Pallas kernels for 0%

profile of v1, /device:TPU:1, one launch (start us, length us, event | category | flops | bytes accessed | tf_op | source)
XLA Modules:
  0.0 287.8 jit_solution(9409759367210519676)
XLA Ops:
  0.6 0.8 reshape.136
  1.4 0.7 reshape.156
  2.2 13.0 %all-to-all-start.1 = ((bf16[64,2,128]{2,1,0:T(2,128)(2,1)}), bf16[64,2,128]{2,1,0:T(2,128)(2,1)S(1)}, u32[]{:S(2)}, u32[]{:S(2)}) async-start(bf16[64,2,128]{2,1,0:T(2,128)(2,1)} %reshape.156), calls=%async_computation.1 | async-start | bytes 65536 | tf_op jit(solution)/shard_map/all_to_all | solution.py:18
  15.2 1.0 multiply_convert_fusion.1
  16.3 8.2 %all-to-all-done.1 = bf16[64,2,128]{2,1,0:T(2,128)(2,1)S(1)} async-done(((bf16[64,2,128]{2,1,0:T(2,128)(2,1)}), bf16[64,2,128]{2,1,0:T(2,128)(2,1)S(1)}, u32[]{:S(2)}, u32[]{:S(2)}) %all-to-all-start.1) | async-done | bytes 32800 | tf_op jit(solution)/shard_map/all_to_all | solution.py:18
  24.5 1.2 stack.7
  25.7 3.7 %all-to-all-start.2 = ((bf16[8,64,1408]{2,1,0:T(8,128)(2,1)}), bf16[8,64,1408]{2,1,0:T(8,128)(2,1)S(1)}, u32[]{:S(2)}, u32[]{:S(2)}) async-start(bf16[8,64,1408]{2,1,0:T(8,128)(2,1)} %stack.7), calls=%async_computation.2 | async-start | bytes 2883584 | tf_op jit(solution)/shard_map/all_to_all | solution.py:141
  29.4 0.7 constant_dynamic-slice_fusion
  31.1 34.1 %all-to-all-done.2 = bf16[8,64,1408]{2,1,0:T(8,128)(2,1)S(1)} async-done(((bf16[8,64,1408]{2,1,0:T(8,128)(2,1)}), bf16[8,64,1408]{2,1,0:T(8,128)(2,1)S(1)}, u32[]{:S(2)}, u32[]{:S(2)}) %all-to-all-start.2) | async-done | bytes 1441824 | tf_op jit(solution)/shard_map/all_to_all | solution.py:141
  65.2 0.4 fusion
  65.6 0.8 broadcast_in_dim.91
  66.4 4.2 %all-to-all-start.3 = ((bf16[4,32,1536]{2,1,0:T(8,128)(2,1)}), bf16[4,32,1536]{2,1,0:T(8,128)(2,1)S(1)}, u32[]{:S(2)}, u32[]{:S(2)}) async-start(bf16[4,32,1536]{2,1,0:T(8,128)(2,1)} %broadcast_in_dim.91), calls=%async_computation.3 | async-start | bytes 786432 | tf_op jit(solution)/shard_map/all_to_all | solution.py:18
  70.7 6.1 %all-to-all-done.3 = bf16[4,32,1536]{2,1,0:T(8,128)(2,1)S(1)} async-done(((bf16[4,32,1536]{2,1,0:T(8,128)(2,1)}), bf16[4,32,1536]{2,1,0:T(8,128)(2,1)S(1)}, u32[]{:S(2)}, u32[]{:S(2)}) %all-to-all-start.3) | async-done | bytes 393248 | tf_op jit(solution)/shard_map/all_to_all | solution.py:18
  76.8 1.6 stack.8
  78.4 3.9 %all-to-all-start.4 = ((bf16[8,64,2368]{2,1,0:T(8,128)(2,1)}), bf16[8,64,2368]{2,1,0:T(8,128)(2,1)S(1)}, u32[]{:S(2)}, u32[]{:S(2)}) async-start(bf16[8,64,2368]{2,1,0:T(8,128)(2,1)} %stack.8), calls=%async_computation.4 | async-start | bytes 4980736 | tf_op jit(solution)/shard_map/all_to_all | solution.py:141
  82.4 0.2 fusion.41
  82.6 57.1 %all-to-all-done.4 = bf16[8,64,2368]{2,1,0:T(8,128)(2,1)S(1)} async-done(((bf16[8,64,2368]{2,1,0:T(8,128)(2,1)}), bf16[8,64,2368]{2,1,0:T(8,128)(2,1)S(1)}, u32[]{:S(2)}, u32[]{:S(2)}) %all-to-all-start.4) | async-done | bytes 2424864 | tf_op jit(solution)/shard_map/all_to_all | solution.py:141
  139.7 0.3 convolution_convert_fusion.3
  140.0 1.1 broadcast_in_dim.93
  141.1 0.1 copy-done.2
  141.2 6.5 %all-to-all-start.5 = ((bf16[8,32,512]{2,1,0:T(8,128)(2,1)}), bf16[8,32,512]{2,1,0:T(8,128)(2,1)S(1)}, u32[]{:S(2)}, u32[]{:S(2)}) async-start(bf16[8,32,512]{2,1,0:T(8,128)(2,1)} %broadcast_in_dim.93), calls=%async_computation.5 | async-start | bytes 524288 | tf_op jit(solution)/shard_map/all_to_all | solution.py:18
  147.9 6.4 %all-to-all-done.5 = bf16[8,32,512]{2,1,0:T(8,128)(2,1)S(1)} async-done(((bf16[8,32,512]{2,1,0:T(8,128)(2,1)}), bf16[8,32,512]{2,1,0:T(8,128)(2,1)S(1)}, u32[]{:S(2)}, u32[]{:S(2)}) %all-to-all-start.5) | async-done | bytes 262176 | tf_op jit(solution)/shard_map/all_to_all | solution.py:18
  154.4 2.2 fusion.3
  156.9 0.7 pad_maximum_fusion.2
  157.5 3.3 %all-to-all-start.6 = ((bf16[4,8,1664]{2,1,0:T(8,128)(2,1)}), bf16[4,8,1664]{2,1,0:T(8,128)(2,1)S(1)}, u32[]{:S(2)}, u32[]{:S(2)}) async-start(bf16[4,8,1664]{2,1,0:T(8,128)(2,1)} %pad_maximum_fusion.2), calls=%async_computation.6 | async-start | bytes 212992 | tf_op jit(solution)/shard_map/all_to_all | solution.py:18
  160.9 4.6 %all-to-all-done.6 = bf16[4,8,1664]{2,1,0:T(8,128)(2,1)S(1)} async-done(((bf16[4,8,1664]{2,1,0:T(8,128)(2,1)}), bf16[4,8,1664]{2,1,0:T(8,128)(2,1)S(1)}, u32[]{:S(2)}, u32[]{:S(2)}) %all-to-all-start.6) | async-done | bytes 106528 | tf_op jit(solution)/shard_map/all_to_all | solution.py:18
  165.5 0.2 fusion.56
  166.3 2.0 fusion.1
  168.4 0.7 multiply_add_fusion
  169.2 1.3 copy-done.1
  170.5 1.9 fusion.65
  172.5 0.6 broadcast_in_dim.98
  173.1 3.3 %all-to-all-start.7 = ((bf16[4,8,512]{2,1,0:T(8,128)(2,1)}), bf16[4,8,512]{2,1,0:T(8,128)(2,1)S(1)}, u32[]{:S(2)}, u32[]{:S(2)}) async-start(bf16[4,8,512]{2,1,0:T(8,128)(2,1)} %broadcast_in_dim.98), calls=%async_computation.7 | async-start | bytes 65536 | tf_op jit(solution)/shard_map/all_to_all | solution.py:18
  176.5 4.2 %all-to-all-done.7 = bf16[4,8,512]{2,1,0:T(8,128)(2,1)S(1)} async-done(((bf16[4,8,512]{2,1,0:T(8,128)(2,1)}), bf16[4,8,512]{2,1,0:T(8,128)(2,1)S(1)}, u32[]{:S(2)}, u32[]{:S(2)}) %all-to-all-start.7) | async-done | bytes 32800 | tf_op jit(solution)/shard_map/all_to_all | solution.py:18
  180.7 0.2 stack.6
  180.9 64.1 %all_to_all.55 = bf16[8,64,2624]{2,1,0:T(8,128)(2,1)S(1)} all-to-all(bf16[8,64,2624]{2,1,0:T(8,128)(2,1)S(1)} %stack.6), channel_id=1, replica_groups=mesh['z'=8,'y'=4,'x'=4,'c'=2] {'z'}, dimensions={0} | all-to-all | bytes 5373952 | tf_op jit(solution)/shard_map/all_to_all | solution.py:141
  245.0 0.2 convolution_convert_fusion.4
  245.3 13.4 %all_to_all.56 = bf16[8,32,512]{2,1,0:T(8,128)(2,1)S(1)} all-to-all(bf16[8,32,512]{2,1,0:T(8,128)(2,1)S(1)} %broadcast_in_dim.99), channel_id=1, replica_groups=mesh['z'=8,'y'=4,'x'=4,'c'=2] {'x','c'}, dimensions={0} | all-to-all | bytes 524288 | tf_op jit(solution)/shard_map/all_to_all | solution.py:18
  258.8 0.3 convolution_convert_fusion
  259.3 0.8 broadcast_in_dim.102
  260.1 3.5 %all-to-all-start.9 = ((bf16[4,32,1536]{2,1,0:T(8,128)(2,1)}), bf16[4,32,1536]{2,1,0:T(8,128)(2,1)S(1)}, u32[]{:S(2)}, u32[]{:S(2)}) async-start(bf16[4,32,1536]{2,1,0:T(8,128)(2,1)} %broadcast_in_dim.102), calls=%async_computation.9 | async-start | bytes 786432 | tf_op jit(solution)/shard_map/all_to_all | solution.py:18
  263.6 6.8 %all-to-all-done.9 = bf16[4,32,1536]{2,1,0:T(8,128)(2,1)S(1)} async-done(((bf16[4,32,1536]{2,1,0:T(8,128)(2,1)}), bf16[4,32,1536]{2,1,0:T(8,128)(2,1)S(1)}, u32[]{:S(2)}, u32[]{:S(2)}) %all-to-all-start.9) | async-done | bytes 393248 | tf_op jit(solution)/shard_map/all_to_all | solution.py:18
  270.4 0.2 fusion.36
  270.6 0.4 convolution_convert_fusion.2
  271.1 0.2 reshape.158
  271.3 15.5 %all_to_all.57 = bf16[64,2,256]{2,1,0:T(2,128)(2,1)S(1)} all-to-all(bf16[64,2,256]{2,1,0:T(2,128)(2,1)S(1)} %reshape.158), channel_id=1, replica_groups=mesh['z'=8,'y'=4,'x'=4,'c'=2] {'z','x','c'}, dimensions={0} | all-to-all | bytes 131072 | tf_op jit(solution)/shard_map/all_to_all | solution.py:18
  286.8 0.1 reshape.159
  287.1 0.7 convert_element_type.213
  (92 shorter events, 3.1 us)
Async XLA Ops:
  2.2 22.3 %all-to-all-start.1 = ((bf16[64,2,128]{2,1,0:T(2,128)(2,1)}), bf16[64,2,128]{2,1,0:T(2,128)(2,1)S(1)}, u32[]{:S(2)}, u32[]{:S(2)}) async-start(bf16[64,2,128]{2,1,0:T(2,128)(2,1)} %reshape.156), calls=%async_computation.1 | async-start | bytes 65536 | tf_op jit(solution)/shard_map/all_to_all | solution.py:18
  16.2 14.2 %copy-start.7 = (bf16[64,512]{1,0:T(8,128)(2,1)S(1)}, bf16[64,512]{1,0:T(8,128)(2,1)}, u32[]{:S(2)}) copy-start(bf16[64,512]{1,0:T(8,128)(2,1)} %param.30) | copy-start | bytes 196612
  16.2 14.2 %copy-start.8 = (bf16[64,512]{1,0:T(8,128)(2,1)S(1)}, bf16[64,512]{1,0:T(8,128)(2,1)}, u32[]{:S(2)}) copy-start(bf16[64,512]{1,0:T(8,128)(2,1)} %param.31) | copy-start | bytes 196612
  16.2 14.2 %copy-start.10 = (bf16[64,256]{1,0:T(8,128)(2,1)S(1)}, bf16[64,256]{1,0:T(8,128)(2,1)}, u32[]{:S(2)}) copy-start(bf16[64,256]{1,0:T(8,128)(2,1)} %param.28) | copy-start | bytes 98308
  16.3 14.2 %copy-start.11 = (bf16[64,256]{1,0:T(8,128)(2,1)S(1)}, bf16[64,256]{1,0:T(8,128)(2,1)}, u32[]{:S(2)}) copy-start(bf16[64,256]{1,0:T(8,128)(2,1)} %param.29) | copy-start | bytes 98308
  25.7 4.8 %copy-start.12 = (f32[64]{0:T(128)S(1)}, f32[64]{0:T(128)}, u32[]{:S(2)}) copy-start(f32[64]{0:T(128)} %param.27) | copy-start | bytes 772
  25.7 39.5 %all-to-all-start.2 = ((bf16[8,64,1408]{2,1,0:T(8,128)(2,1)}), bf16[8,64,1408]{2,1,0:T(8,128)(2,1)S(1)}, u32[]{:S(2)}, u32[]{:S(2)}) async-start(bf16[8,64,1408]{2,1,0:T(8,128)(2,1)} %stack.7), calls=%async_computation.2 | async-start | bytes 2883584 | tf_op jit(solution)/shard_map/all_to_all | solution.py:141
  30.4 40.1 %copy-start.3 = (bf16[704,64]{0,1:T(8,128)(2,1)S(1)}, bf16[704,64]{0,1:T(8,128)(2,1)}, u32[]{:S(2)}) copy-start(bf16[704,64]{0,1:T(8,128)(2,1)} %param.26) | copy-start | bytes 270340
  66.4 10.4 %all-to-all-start.3 = ((bf16[4,32,1536]{2,1,0:T(8,128)(2,1)}), bf16[4,32,1536]{2,1,0:T(8,128)(2,1)S(1)}, u32[]{:S(2)}, u32[]{:S(2)}) async-start(bf16[4,32,1536]{2,1,0:T(8,128)(2,1)} %broadcast_in_dim.91), calls=%async_computation.3 | async-start | bytes 786432 | tf_op jit(solution)/shard_map/all_to_all | solution.py:18
  78.4 61.3 %all-to-all-start.4 = ((bf16[8,64,2368]{2,1,0:T(8,128)(2,1)}), bf16[8,64,2368]{2,1,0:T(8,128)(2,1)S(1)}, u32[]{:S(2)}, u32[]{:S(2)}) async-start(bf16[8,64,2368]{2,1,0:T(8,128)(2,1)} %stack.8), calls=%async_computation.4 | async-start | bytes 4980736 | tf_op jit(solution)/shard_map/all_to_all | solution.py:141
  82.3 65.5 %copy-start.4 = (bf16[64,704]{1,0:T(8,128)(2,1)S(1)}, bf16[64,704]{1,0:T(8,128)(2,1)}, u32[]{:S(2)}) copy-start(bf16[64,704]{1,0:T(8,128)(2,1)} %param.40) | copy-start | bytes 270340
  82.3 65.5 %copy-start.5 = (bf16[64,704]{1,0:T(8,128)(2,1)S(1)}, bf16[64,704]{1,0:T(8,128)(2,1)}, u32[]{:S(2)}) copy-start(bf16[64,704]{1,0:T(8,128)(2,1)} %param.39) | copy-start | bytes 270340
  82.3 65.4 %copy-start.13 = (f32[64]{0:T(128)S(1)}, f32[64]{0:T(128)}, u32[]{:S(2)}) copy-start(f32[64]{0:T(128)} %param.38) | copy-start | bytes 772
  139.7 1.6 copy-start.2
  141.1 19.8 %copy-start.16 = (f32[4]{0:T(128)S(1)}, f32[4]{0:T(128)}, u32[]{:S(2)}) copy-start(f32[4]{0:T(128)} %param.34) | copy-start | bytes 52
  141.1 24.9 %copy-start.15 = (f32[4]{0:T(128)S(1)}, f32[4]{0:T(128)}, u32[]{:S(2)}) copy-start(f32[4]{0:T(128)} %param.35) | copy-start | bytes 52
  141.2 13.0 %all-to-all-start.5 = ((bf16[8,32,512]{2,1,0:T(8,128)(2,1)}), bf16[8,32,512]{2,1,0:T(8,128)(2,1)S(1)}, u32[]{:S(2)}, u32[]{:S(2)}) async-start(bf16[8,32,512]{2,1,0:T(8,128)(2,1)} %broadcast_in_dim.93), calls=%async_computation.5 | async-start | bytes 524288 | tf_op jit(solution)/shard_map/all_to_all | solution.py:18
  147.8 18.5 %copy-start = (f32[8,4,128,128]{3,2,1,0:T(8,128)S(1)}, f32[8,4,128,128]{3,2,1,0:T(8,128)}, u32[]{:S(2)}) copy-start(f32[8,4,128,128]{3,2,1,0:T(8,128)} %param.22) | copy-start | bytes 6291460
  157.5 8.0 %all-to-all-start.6 = ((bf16[4,8,1664]{2,1,0:T(8,128)(2,1)}), bf16[4,8,1664]{2,1,0:T(8,128)(2,1)S(1)}, u32[]{:S(2)}, u32[]{:S(2)}) async-start(bf16[4,8,1664]{2,1,0:T(8,128)(2,1)} %pad_maximum_fusion.2), calls=%async_computation.6 | async-start | bytes 212992 | tf_op jit(solution)/shard_map/all_to_all | solution.py:18
  169.1 1.3 copy-start.1
  169.2 3.3 %copy-start.14 = (f32[128]{0:T(128)S(1)}, f32[128]{0:T(128)}, u32[]{:S(2)}) copy-start(f32[128]{0:T(128)} %param.36) | copy-start | bytes 1540
  169.2 7.2 %copy-start.6 = (bf16[704,64]{0,1:T(8,128)(2,1)S(1)}, bf16[704,64]{0,1:T(8,128)(2,1)}, u32[]{:S(2)}) copy-start(bf16[704,64]{0,1:T(8,128)(2,1)} %param.41) | copy-start | bytes 270340
  169.2 7.2 %copy-start.9 = (bf16[512,64]{0,1:T(8,128)(2,1)S(1)}, bf16[512,64]{0,1:T(8,128)(2,1)}, u32[]{:S(2)}) copy-start(bf16[512,64]{0,1:T(8,128)(2,1)} %param.37) | copy-start | bytes 196612
  173.1 7.5 %all-to-all-start.7 = ((bf16[4,8,512]{2,1,0:T(8,128)(2,1)}), bf16[4,8,512]{2,1,0:T(8,128)(2,1)S(1)}, u32[]{:S(2)}, u32[]{:S(2)}) async-start(bf16[4,8,512]{2,1,0:T(8,128)(2,1)} %broadcast_in_dim.98), calls=%async_computation.7 | async-start | bytes 65536 | tf_op jit(solution)/shard_map/all_to_all | solution.py:18
  260.1 10.3 %all-to-all-start.9 = ((bf16[4,32,1536]{2,1,0:T(8,128)(2,1)}), bf16[4,32,1536]{2,1,0:T(8,128)(2,1)S(1)}, u32[]{:S(2)}, u32[]{:S(2)}) async-start(bf16[4,32,1536]{2,1,0:T(8,128)(2,1)} %broadcast_in_dim.102), calls=%async_computation.9 | async-start | bytes 786432 | tf_op jit(solution)/shard_map/all_to_all | solution.py:18
